TPU v7x, 256 devices: a whole 4x4x8 slice. The times are simulated.
256 devices in a mesh: ep: 16 (over y, x), tp: 16 (over z, core).
Axes of the slice: x: 4, y: 4, z: 8, core: 2. Of those that a mesh axis runs over, the one named last changes fastest.
Arguments:
- query_preactivation: bfloat16 [32768, 2048], P('ep', 'tp'), may hold values from -6 to 6
- forget_preactivation: bfloat16 [32768, 2048], P('ep', 'tp'), may hold values from -6 to 6
- value_input_rows: bfloat16 [32768, 1024], P('ep', 'tp'), may hold values from -8 to 8
- output_gate_preactivation: bfloat16 [32768, 1024], P('ep', 'tp'), may hold values from -6 to 6
- forget_floor_gap: float32 [2048], P('tp'), may hold values from 0 to 0.2, as said below
- extra_log_forget: float32 [32768, 16], P('ep', 'tp'), may hold values from -2 to 0
- head_output_gain: float32 [1024], P('tp'), may hold values from 0.1 to 1.9
- mixer_output_weight: bfloat16 [1024, 2048], P(None, 'tp'), may hold values from -0.1875 to 0.1875
- second_batch_tokens: bfloat16 [8192, 2048], P('ep'), may hold values from -6 to 6
- feedforward_norm_gain: float32 [2048], replicated, may hold values from 0.1 to 1.9
- chosen_expert_index: int32 [8192, 2], P('ep'), may hold values from 0 to 15, all different within a row; in each aligned block of 32 rows (0 to 31, 32 to 63, ...) at most 5 rows name the same one
- chosen_expert_weight: float32 [8192, 2], P('ep'), may hold values from 0.1 to 1
- expert_gate_weight: bfloat16 [16, 2048, 7168], P('ep', None, 'tp'), may hold values from -0.125 to 0.125
- expert_up_weight: bfloat16 [16, 2048, 7168], P('ep', None, 'tp'), may hold values from -0.125 to 0.125
- expert_down_weight: bfloat16 [16, 7168, 2048], P('ep', 'tp'), may hold values from -0.0625 to 0.0625
Outputs:
- mixer_output_first: bfloat16 [32768, 2048], P('ep', 'tp')
- moe_out: bfloat16 [8192, 2048], P(('ep', 'tp'))
Inputs may be any that keep to these rules, and one draw needn't show every extreme that they name: `chosen_expert_index`: each row names 2 different experts. In each aligned block of 32 rows (the rows of one device's share) no expert is named by more than 5 rows, and in every draw some expert is named by exactly 5 rows of some block. `forget_floor_gap`: every entry is positive.
All inputs are finite; a program needn't handle non-finite values.
Results may differ from a plain program's by a relative error of at most 0.019.
Values may be sent and summed in bfloat16 or wider, within the bound.
A program may use at most 128 MiB of HBM per device.

v0:
```python
import jax
import jax.numpy as jnp
from jax import lax
from jax.sharding import PartitionSpec as P

KEY_DIM = 128
VAL_DIM = 64
BLOCK_POSITIONS = 64
TOPK = 2
epsilon = 1e-06


def copy_for_each(shard, axis):
    copies = jnp.broadcast_to(shard, (lax.axis_size(axis), *shard.shape))
    return lax.all_to_all(copies, axis, split_axis=0, concat_axis=0, tiled=True)


def all_in_one(shard, axis):
    leaves = jax.tree.leaves(shard)
    sequence = sorted(range(len(leaves)), key=lambda k: -leaves[k].size)
    width = (1, *leaves[sequence[0]].shape)[-1]
    lines = [
        jnp.pad(leaves[k].reshape(-1), (0, -leaves[k].size % width)).reshape(-1, width)
        for k in sequence
    ]
    both, at, found = (copy_for_each(jnp.concatenate(lines), axis), 0, {})
    for k, line in zip(sequence, lines):
        slab = both[:, at : at + len(line)].reshape(len(both), -1)
        found[k] = slab[:, : leaves[k].size].reshape(-1, *leaves[k].shape)
        at += len(line)
    numbers = iter(range(len(leaves)))
    return jax.tree.map(lambda _: found[next(numbers)], shard)


def combined_pairwise(pieces, combine):
    while len(jax.tree.leaves(pieces)[0]) > 1:
        pieces = jax.vmap(combine)(
            *(jax.tree.map(lambda part: part[side::2], pieces) for side in (0, 1))
        )
    return jax.tree.map(lambda part: part[0], pieces)


def carried_in(shard, axis, combine, identity):
    count, here = (lax.axis_size(axis), lax.axis_index(axis))
    passed = jnp.arange(count) < here

    def kept(part, zero, own):
        part = jnp.where(
            passed.reshape(-1, *(1 for _ in own.shape)),
            part.astype(own.dtype),
            jnp.asarray(zero, own.dtype),
        )
        return part

    pieces = all_in_one(
        jax.tree.map(lambda part, kind: part.astype(kind), shard, (jnp.bfloat16, jnp.bfloat16)),
        axis,
    )
    return combined_pairwise(jax.tree.map(kept, pieces, identity, shard), combine)


def combine_states(earlier, later):
    return (earlier[0] * later[0], later[0][..., None] * earlier[1] + later[1])


def norm_rows(tokens, row_gain):
    tokens_float = tokens.astype(jnp.float32)
    factor = lax.rsqrt(jnp.mean(tokens_float * tokens_float, axis=-1, keepdims=True) + epsilon)
    return (tokens_float * factor * row_gain).astype(jnp.bfloat16)


def slot_positions(blocks, experts_all):
    flattened = blocks.reshape(blocks.shape[0], -1)
    onehot = (flattened[..., None] == jnp.arange(experts_all, dtype=jnp.int32)).astype(jnp.int32)
    earlier = jnp.cumsum(onehot, axis=1) - onehot
    return jnp.sum(earlier * onehot, axis=-1).reshape(blocks.shape)


def fill_slots(rows_in, blocks, slot_ids, experts_all, capacity):
    groups = blocks.shape[0]
    sub_rows = blocks.shape[1]
    group_ids = jnp.arange(groups, dtype=jnp.int32)[:, None, None]
    target = (group_ids * experts_all + blocks) * capacity + slot_ids
    sources = jnp.broadcast_to(
        jnp.arange(sub_rows, dtype=jnp.int32)[None, :, None] + group_ids * sub_rows, blocks.shape
    )
    lookup = (
        jnp.full((groups * experts_all * capacity,), -1, jnp.int32)
        .at[target.reshape(-1)]
        .set(sources.reshape(-1))
    )
    gathered = rows_in.reshape(groups * sub_rows, -1)[jnp.maximum(lookup, 0)]
    filled = jnp.where((lookup >= 0)[:, None], gathered, jnp.zeros((), gathered.dtype))
    return filled.reshape(groups, experts_all, capacity, -1)


def on_device(
    query_preactivation,
    forget_preactivation,
    value_input_rows,
    output_gate_preactivation,
    forget_floor_gap,
    extra_log_forget,
    head_output_gain,
    mixer_output_weight,
    second_batch_tokens,
    feedforward_norm_gain,
    chosen_expert_index,
    chosen_expert_weight,
    expert_gate_weight,
    expert_up_weight,
    expert_down_weight,
):
    length = query_preactivation.shape[0]
    device_heads = forget_floor_gap.shape[0] // KEY_DIM
    block_count = length // BLOCK_POSITIONS
    shape_key = (block_count, BLOCK_POSITIONS, device_heads, KEY_DIM)
    queries = jax.nn.silu(query_preactivation.astype(jnp.float32)).reshape(shape_key)
    key_decay_rates = forget_floor_gap.reshape(device_heads, KEY_DIM) * jax.nn.sigmoid(
        -forget_preactivation.astype(jnp.float32)
    ).reshape(shape_key)
    forget_log_factor = (
        jnp.log(1.0 - key_decay_rates)
        + extra_log_forget.reshape(block_count, BLOCK_POSITIONS, device_heads)[..., None]
    )
    values = value_input_rows.astype(jnp.float32).reshape(
        block_count, BLOCK_POSITIONS, device_heads, VAL_DIM
    )
    cumulative_log = jnp.cumsum(forget_log_factor, axis=1)
    block_final_row = cumulative_log[:, -1]
    query_scaled = queries * jnp.exp(cumulative_log - block_final_row[:, None])
    scaled_key_rows = key_decay_rates * jnp.exp(block_final_row[:, None] - cumulative_log)
    scores = jnp.einsum("nthk,nshk->nhts", query_scaled, scaled_key_rows)
    causal_mask = jnp.arange(BLOCK_POSITIONS)[:, None] >= jnp.arange(BLOCK_POSITIONS)[None, :]
    scores = jnp.where(causal_mask, scores, 0.0)
    within = jnp.einsum("nhts,nshv->nthv", scores, values)
    updates = jnp.einsum("nshk,nshv->nhkv", scaled_key_rows, values)
    decays = jnp.exp(block_final_row)
    run_decay, run_state = lax.associative_scan(combine_states, (decays, updates))
    carried = carried_in(
        (run_decay[-1], run_state[-1]),
        "ep",
        combine_states,
        (jnp.ones_like(decays[0]), jnp.zeros_like(updates[0])),
    )
    prior_decay = jnp.concatenate([jnp.ones_like(decays[:1]), run_decay[:-1]], axis=0)
    prior_state = jnp.concatenate([jnp.zeros_like(updates[:1]), run_state[:-1]], axis=0)
    prior_full = prior_state + prior_decay[..., None] * carried[1][None]
    across_blocks = jnp.einsum("nthk,nhkv->nthv", queries * jnp.exp(cumulative_log), prior_full)
    recurrent = (within + across_blocks).reshape(length, device_heads, VAL_DIM)
    factor = lax.rsqrt(jnp.mean(recurrent * recurrent, axis=-1, keepdims=True) + epsilon)
    normed = (recurrent * factor * head_output_gain.reshape(device_heads, VAL_DIM)).reshape(
        length, device_heads * VAL_DIM
    )
    mixed = (normed * jax.nn.silu(output_gate_preactivation.astype(jnp.float32))).astype(
        jnp.bfloat16
    )
    mixer_output_first = jnp.dot(
        lax.all_gather(mixed, "tp", axis=1, tiled=True),
        mixer_output_weight,
        preferred_element_type=jnp.float32,
    ).astype(jnp.bfloat16)
    local_experts = expert_gate_weight.shape[0]
    experts_all = local_experts * lax.axis_size("ep")
    groups = lax.axis_size("tp")
    sub_rows = second_batch_tokens.shape[0] // groups
    capacity = max(2, sub_rows * TOPK * 5 // (4 * experts_all))
    position = lax.axis_index("tp")
    own_routes = lax.dynamic_slice_in_dim(chosen_expert_index, position * sub_rows, sub_rows, 0)
    own_weights = lax.dynamic_slice_in_dim(chosen_expert_weight, position * sub_rows, sub_rows, 0)
    own_slots = slot_positions(own_routes[None], experts_all)[0]
    own_rows = lax.dynamic_slice_in_dim(second_batch_tokens, position * sub_rows, sub_rows, 0)
    outgoing = fill_slots(
        norm_rows(own_rows, feedforward_norm_gain)[None],
        own_routes[None],
        own_slots[None],
        experts_all,
        capacity,
    )[0]
    arrived = lax.all_to_all(outgoing, "ep", split_axis=0, concat_axis=0, tiled=True)
    segment = lax.all_gather(arrived[None], "tp", axis=0, tiled=True)
    shaped = segment.reshape(segment.shape[0], -1, local_experts, capacity, segment.shape[-1])
    gate_part = jnp.einsum(
        "tsecd,edf->tsecf", shaped, expert_gate_weight, preferred_element_type=jnp.float32
    )
    up_part = jnp.einsum(
        "tsecd,edf->tsecf", shaped, expert_up_weight, preferred_element_type=jnp.float32
    )
    hidden = (jax.nn.silu(gate_part) * up_part).astype(jnp.bfloat16)
    rows_each = hidden.shape[1] * hidden.shape[2] * hidden.shape[3]
    product = jnp.einsum(
        "tsecf,efd->tsecd", hidden, expert_down_weight, preferred_element_type=jnp.float32
    )
    summed = lax.psum_scatter(
        product.reshape(rows_each * lax.axis_size("tp"), product.shape[-1]).astype(jnp.bfloat16),
        "tp",
        scatter_dimension=0,
        tiled=True,
    ).astype(jnp.float32)
    to_return = summed.astype(jnp.bfloat16).reshape(-1, local_experts * capacity, summed.shape[-1])
    returned = lax.all_to_all(to_return, "ep", split_axis=0, concat_axis=0, tiled=True)
    results = returned.reshape(experts_all * capacity, -1)
    flat_index = own_routes * capacity + own_slots
    combined = jnp.zeros((sub_rows, results.shape[1]), jnp.float32)
    for ranked in range(TOPK):
        combined = (
            combined
            + results[flat_index[:, ranked]].astype(jnp.float32)
            * own_weights[:, ranked : ranked + 1]
        )
    return (mixer_output_first, combined.astype(jnp.bfloat16))


def solution(mesh):
    placed = (
        P("ep", "tp"),
        P("ep", "tp"),
        P("ep", "tp"),
        P("ep", "tp"),
        P("tp"),
        P("ep", "tp"),
        P("tp"),
        P(None, "tp"),
        P("ep", None),
        P(),
        P("ep", None),
        P("ep", None),
        P("ep", None, "tp"),
        P("ep", None, "tp"),
        P("ep", "tp", None),
    )
    return jax.shard_map(
        on_device,
        mesh=mesh,
        in_specs=placed,
        out_specs=(P("ep", "tp"), P(("ep", "tp"), None)),
        check_vma=False,
    )
```

profile of v0, /device:TPU:1, one launch (start us, length us, event | category | flops | bytes accessed | tf_op | source)
XLA Modules:
  0.0 234.6 jit_solution(4051905095843440140)
XLA Ops:
  7.2 0.9 constant_dynamic-slice_fusion.1
  8.1 0.1 copy.139
  8.2 0.1 eq.27
  8.4 0.1 reduce_window_sum.26
  8.5 0.2 select_reduce_fusion
  8.7 0.1 broadcast_in_dim_squeeze_reshape.3
  8.8 0.1 reshape.456
  8.9 0.1 reshape.492
  9.0 0.8 scatter_custom_fusion
  9.8 1.0 fusion.61
  10.9 1.0 fusion.63
  11.9 0.8 gather_fusion
  12.8 0.1 gather.12
  13.0 0.1 broadcast_select_fusion
  13.1 17.8 %all_to_all.15 = bf16[16,5,2048]{2,1,0:T(8,128)(2,1)S(1)} all-to-all(bf16[16,5,2048]{2,1,0:T(8,128)(2,1)S(1)} %broadcast_select_fusion), channel_id=1, replica_groups=mesh['ep'=16,'tp'=16] {'ep'}, dimensions={0} | all-to-all | bytes 655360 | tf_op jit(solution)/shard_map/all_to_all | solution.py:180
  30.9 0.9 copy.131
  31.9 0.5 broadcast.311
  32.4 0.7 reduce.14
  33.3 0.3 add_divide_fusion
  33.6 42.5 %all-gather.6.cloned.1.call-done = bf16[256,5,2048]{2,0,1:T(8,128)(2,1)} async-done(((bf16[16,5,2048]{2,0,1:T(8,128)(2,1)}), bf16[256,5,2048]{2,0,1:T(8,128)(2,1)}) %all-gather.6.cloned.1.call-update) | async-done | bytes 5242896 | tf_op jit(solution)/shard_map/all_gather | solution.py:181
  76.1 7.5 %fusion = f32[16,16,5,448]{3,1,2,0:T(8,128)} fusion(bf16[16,16,5,2048]{3,1,0,2:T(8,128)(2,1)} %bitcast.161, bf16[1,2048,448]{1,2,0:T(8,128)(2,1)} %param.28), kind=kOutput, calls=%fused_computation.5 | convolution fusion | flops 2348810240 | bytes 9371648 | tf_op jit(solution)/shard_map/tsecd,edf->tsecf/dot_general | solution.py:186
  83.6 10.4 %convert_bitcast_fusion = bf16[16,16,1,5,2048]{4,1,3,0,2:T(8,128)(2,1)} fusion(bf16[1,448,2048]{2,1,0:T(8,128)(2,1)S(1)} %copy-done, f32[16,16,5,448]{3,1,2,0:T(8,128)} %fusion, bf16[16,16,5,2048]{3,1,0,2:T(8,128)(2,1)} %bitcast.162, bf16[1,2048,448]{1,2,0:T(8,128)(2,1)} %param.27), kind=kOutput, calls=%fused_computation.4 | convolution fusion | flops 4703682560 | bytes 16449536 | tf_op jit(solution)/shard_map/tsecf,efd->tsecd/dot_general | solution.py:191
  94.0 10.3 %copy.134 = bf16[16,16,1,5,2048]{4,3,1,0,2:T(8,128)(2,1)} copy(bf16[16,16,1,5,2048]{4,1,3,0,2:T(8,128)(2,1)} %convert_bitcast_fusion) | data formatting | bytes 10485760 | tf_op jit(solution)/shard_map/convert_element_type | solution.py:195
  104.3 10.0 %convert_element_type.116 = bf16[1280,2048]{1,0:T(8,128)(2,1)} reshape(bf16[16,16,1,5,2048]{4,3,1,0,2:T(8,128)(2,1)} %copy.134) | data formatting | bytes 10485760 | tf_op jit(solution)/shard_map/convert_element_type | solution.py:195
  114.4 0.6 copy-done.12
  115.0 0.8 fusion.37
  116.0 0.5 slice_multiply_fusion.4
  116.5 0.6 fusion.84
  117.4 0.1 copy.124
  117.5 0.5 reshape.453
  118.0 0.3 convert_multiply_fusion
  118.3 2.3 fusion.30
  120.6 0.4 fusion.42
  121.0 0.4 copy-done.4
  122.0 0.1 pad.71
  122.1 0.1 pad.70
  122.3 5.9 %pad.149 = f32[31,1,128,64]{2,3,0,1:T(8,128)} pad(f32[16,1,128,64]{2,3,0,1:T(8,128)S(1)} %add.235, f32[]{:T(128)} %constant.15.clone.1), padding=0_0_1x0_0_0x0_0_0x0_0_0 | pad | bytes 1540100
  128.2 0.8 fusion.71
  129.0 0.9 broadcast_in_dim.57
  129.8 6.6 %all-to-all-start = ((bf16[16,130,64]{1,2,0:T(8,128)(2,1)}), bf16[16,130,64]{1,2,0:T(8,128)(2,1)}, u32[]{:S(2)}, u32[]{:S(2)}) async-start(bf16[16,130,64]{1,2,0:T(8,128)(2,1)} %broadcast_in_dim.57), calls=%async_computation | async-start | bytes 1048576 | tf_op jit(solution)/shard_map/all_to_all | solution.py:15
  136.5 6.1 %pad.73 = f32[32,1,128,64]{2,3,0,1:T(8,128)} pad(f32[16,1,128,64]{2,3,0,1:T(8,128)S(1)} %add.235, f32[]{:T(128)} %constant.15.clone.1), padding=1_0_1x0_0_0x0_0_0x0_0_0 | pad | bytes 1572868 | tf_op jit(solution)/shard_map/pad | solution.py:139
  142.7 0.1 fusion.58
  142.8 0.8 pad_maximum_fusion
  143.7 6.2 %pad.72 = f32[32,1,128,64]{2,3,0,1:T(8,128)S(1)} pad(f32[16,1,128,64]{2,3,0,1:T(8,128)} %pad_maximum_fusion, f32[]{:T(128)} %constant.15.clone.1), padding=0_1_1x0_0_0x0_0_0x0_0_0 | pad | bytes 1572868 | tf_op jit(solution)/shard_map/pad | solution.py:139
  149.9 1.1 slice_add_fusion
  151.0 2.0 convolution_bitcast_fusion
  153.1 1.0 slice.331
  154.0 0.2 copy.138
  154.5 1.1 select_bitcast_fusion
  155.7 0.5 multiply_reduce_fusion
  156.3 0.6 copy.129
  156.9 0.4 reshape.455
  157.4 0.9 fusion.56
  158.3 0.8 constant_dynamic-slice_fusion
  159.0 0.2 fusion.72
  159.2 16.0 %reduce-scatter.2.cloned.1.call-done = bf16[80,2048]{1,0:T(8,128)(2,1)} async-done(((bf16[1280,2048]{1,0:T(8,128)(2,1)}), bf16[80,2048]{1,0:T(8,128)(2,1)}) %reduce-scatter.2.cloned.1.call-update) | async-done | bytes 327696 | tf_op jit(solution)/shard_map/reduce_scatter | solution.py:194
  175.2 1.9 reshape.461
  177.1 6.3 %all-to-all-start.2 = ((bf16[16,5,2048]{2,1,0:T(8,128)(2,1)}), bf16[16,5,2048]{2,1,0:T(8,128)(2,1)S(1)}, u32[]{:S(2)}, u32[]{:S(2)}) async-start(bf16[16,5,2048]{2,1,0:T(8,128)(2,1)} %reshape.461), calls=%async_computation.3 | async-start | bytes 1048576 | tf_op jit(solution)/shard_map/all_to_all | solution.py:201
  183.4 38.0 %all-gather.4.cloned.1.call-done = bf16[2048,1024]{0,1:T(8,128)(2,1)} async-done(((bf16[2048,64]{0,1:T(8,128)(2,1)}), bf16[2048,1024]{0,1:T(8,128)(2,1)}) %all-gather.4.cloned.1.call-update) | async-done | bytes 4194320 | tf_op jit(solution)/shard_map/all_gather | solution.py:159
  221.4 4.4 %convolution_convert_fusion = bf16[2048,128]{1,0:T(8,128)(2,1)} fusion(bf16[2048,1024]{0,1:T(8,128)(2,1)} %all-gather.4.cloned.1.call-done, bf16[1024,128]{1,0:T(8,128)(2,1)S(1)} %copy-done.16), kind=kOutput, calls=%fused_computation.16 | convolution fusion | flops 537133056 | bytes 4980736 | tf_op jit(solution)/shard_map/dot_general | solution.py:158
  225.8 0.1 reshape.462
  226.0 0.7 gather_fusion.1
  226.6 0.7 gather_fusion.2
  227.3 0.8 add_convert_fusion
  (140 shorter events, 2.1 us)
Async XLA Ops:
  7.2 76.4 %copy-start = (bf16[1,448,2048]{2,1,0:T(8,128)(2,1)S(1)}, bf16[1,448,2048]{2,1,0:T(8,128)(2,1)}, u32[]{:S(2)}) copy-start(bf16[1,448,2048]{2,1,0:T(8,128)(2,1)} %param.29) | copy-start | bytes 5505028
  7.2 68.9 %all-gather.6.cloned.1.call-start = ((), (), s32[]{:S(2)}) async-start(), calls=%async_computation.6 | async-start | bytes 5570560 | tf_op jit(solution)/shard_map/all_gather | solution.py:181
  12.7 19.7 %copy-start.11 = (f32[2048,1]{0,1:T(1,128)S(1)}, f32[2048,1]{0,1:T(1,128)}, u32[]{:S(2)}) copy-start(f32[2048,1]{0,1:T(1,128)} %param.20) | copy-start | bytes 24580
  12.7 20.5 %copy-start.7 = (bf16[2048,128]{1,0:T(8,128)(2,1)S(1)}, bf16[2048,128]{1,0:T(8,128)(2,1)}, u32[]{:S(2)}) copy-start(bf16[2048,128]{1,0:T(8,128)(2,1)} %param.16) | copy-start | bytes 1572868
  31.9 143.3 %reduce-scatter.2.cloned.1.call-start = ((), (), s32[]{:S(2)}) async-start(), calls=%async_computation.5 | async-start | bytes 5570560 | tf_op jit(solution)/shard_map/reduce_scatter | solution.py:194
  114.3 0.7 copy-start.12
  114.3 3.2 %copy-start.9 = (bf16[2048,64]{0,1:T(8,128)(2,1)S(1)}, bf16[2048,64]{0,1:T(8,128)(2,1)}, u32[]{:S(2)}) copy-start(bf16[2048,64]{0,1:T(8,128)(2,1)} %param.17) | copy-start | bytes 786436
  114.3 3.7 %copy-start.8 = (bf16[2048,128]{1,0:T(8,128)(2,1)S(1)}, bf16[2048,128]{1,0:T(8,128)(2,1)}, u32[]{:S(2)}) copy-start(bf16[2048,128]{1,0:T(8,128)(2,1)} %param.15) | copy-start | bytes 1572868
  118.0 2.6 %copy-start.6 = (bf16[32,64,64]{1,0,2:T(8,128)(2,1)}, bf16[32,64,64]{1,0,2:T(8,128)(2,1)S(1)}, u32[]{:S(2)}) copy-start(bf16[32,64,64]{1,0,2:T(8,128)(2,1)S(1)} %reshape.453) | copy-start | bytes 786436
  120.6 0.8 copy-start.4
  120.6 1.0 copy-start.13
  120.6 1.0 copy-start.14
  129.8 23.2 %all-to-all-start = ((bf16[16,130,64]{1,2,0:T(8,128)(2,1)}), bf16[16,130,64]{1,2,0:T(8,128)(2,1)}, u32[]{:S(2)}, u32[]{:S(2)}) async-start(bf16[16,130,64]{1,2,0:T(8,128)(2,1)} %broadcast_in_dim.57), calls=%async_computation | async-start | bytes 1048576 | tf_op jit(solution)/shard_map/all_to_all | solution.py:15
  136.4 85.0 %all-gather.4.cloned.1.call-start = ((), (), s32[]{:S(2)}) async-start(), calls=%async_computation.4 | async-start | bytes 4456448 | tf_op jit(solution)/shard_map/all_gather | solution.py:159
  142.8 7.1 %copy-start.2 = (f32[32,1,128,64]{2,3,0,1:T(8,128)S(1)}, f32[32,1,128,64]{2,3,0,1:T(8,128)}, u32[]{:S(2)}) copy-start(f32[32,1,128,64]{2,3,0,1:T(8,128)} %pad.73) | copy-start | bytes 3145732
  142.8 8.2 %copy-start.5 = (bf16[32,64,128]{2,0,1:T(8,128)(2,1)S(1)}, bf16[32,64,128]{2,0,1:T(8,128)(2,1)}, u32[]{:S(2)}) copy-start(bf16[32,64,128]{2,0,1:T(8,128)(2,1)} %copy-done.4) | copy-start | bytes 1572868
  151.0 4.7 %copy-start.3 = (f32[31,1,128,64]{2,3,0,1:T(8,128)S(1)}, f32[31,1,128,64]{2,3,0,1:T(8,128)}, u32[]{:S(2)}) copy-start(f32[31,1,128,64]{2,3,0,1:T(8,128)} %slice_add_fusion) | copy-start | bytes 3047428
  156.2 1.1 copy-start.10
  156.3 1.1 copy-start.15
  156.9 64.5 %copy-start.16 = (bf16[1024,128]{1,0:T(8,128)(2,1)S(1)}, bf16[1024,128]{1,0:T(8,128)(2,1)}, u32[]{:S(2)}) copy-start(bf16[1024,128]{1,0:T(8,128)(2,1)} %param.22) | copy-start | bytes 786436
  177.1 48.7 %all-to-all-start.2 = ((bf16[16,5,2048]{2,1,0:T(8,128)(2,1)}), bf16[16,5,2048]{2,1,0:T(8,128)(2,1)S(1)}, u32[]{:S(2)}, u32[]{:S(2)}) async-start(bf16[16,5,2048]{2,1,0:T(8,128)(2,1)} %reshape.461), calls=%async_computation.3 | async-start | bytes 1048576 | tf_op jit(solution)/shard_map/all_to_all | solution.py:201
  221.4 6.7 %copy-start.1 = (bf16[1,448,2048]{2,1,0:T(8,128)(2,1)S(1)}, bf16[1,448,2048]{2,1,0:T(8,128)(2,1)}, u32[]{:S(2)}) copy-start(bf16[1,448,2048]{2,1,0:T(8,128)(2,1)} %param.29) | copy-start | bytes 5505028
Sparse Core Ops, SparseCore 0:
  32.0 44.0 all-gather.5
  114.5 60.6 reduce-scatter.1
  177.6 43.7 all-gather.3
where the time goes:
time: 236 us; the launch traced here: 235 us
  waiting for transfers between devices  96.6 us (41%)
  local copies, waits for them, and re-layouts  53.1 us (22%)
  matrix products  25.2 us (11%)
  blocking collectives  17.8 us (8%)
  between operations  14.5 us (6%)
  other arithmetic  14.4 us (6%)
  starting transfers between devices  13 us (6%)
    all_gather x1, waiting for transfers between devices, on_device(): segment = lax.all_gather(arrived[None], 'tp', axis=0, tiled=True)  42.5 us
    all_gather x1, waiting for transfers between devices, on_device(): lax.all_gather(mixed, 'tp', axis=1, tiled=True)  38 us
    convert_element_type x2, local copies, waits for them, and re-layouts, on_device(): product.reshape(rows_each * lax.axis_size('tp'), product.shape[-1])  20.4 us
    all_to_all x1, blocking collectives, on_device(): lax.all_to_all(outgoing, 'ep', split_axis=0, concat_axis=0, tiled=True)  17.8 us
    reduce_scatter x1, waiting for transfers between devices, on_device(): lax.psum_scatter(product.reshape(rows_each * lax.axis_size('tp'), product...  16 us
    pad x16, local copies, waits for them, and re-layouts, on_device(): lax.associative_scan(combine_states, (decays, updates))  12.7 us
    dot_general x1, matrix products, on_device(): jnp.einsum('tsecf,efd->tsecd', hidden, expert_down_weight, preferred_elem...  10.4 us
    unnamed x39, local copies, waits for them, and re-layouts  7.75 us
  transfers between devices with their start and end apart: 5, of which 3 were waited for; matrix products, arithmetic and copies ran while one was open for 19% of the time, Pallas kernels for 0%

commit v1 on v0

--- a/solution.py
+++ b/solution.py
@@ -156,7 +156,7 @@
         jnp.bfloat16
     )
     mixer_output_first = jnp.dot(
-        lax.all_gather(mixed, "tp", axis=1, tiled=True),
+        jnp.concatenate(lax.all_gather(mixed, "tp"), axis=1),
         mixer_output_weight,
         preferred_element_type=jnp.float32,
     ).astype(jnp.bfloat16)

time: 236 us -> 251 us (1.064)
  the two profiles are of different devices: /device:TPU:1 before, /device:TPU:2 now
where the time goes in v1:
time: 251 us; the launch traced here: 248 us
  local copies, waits for them, and re-layouts  80.3 us (32%)
  waiting for transfers between devices  76.3 us (30%)
  other arithmetic  30.4 us (12%)
  matrix products  26.5 us (11%)
  starting transfers between devices  20.3 us (8%)
  between operations  14.5 us (6%)
    reduce_scatter x1, waiting for transfers between devices, on_device(): lax.psum_scatter(product.reshape(rows_each * lax.axis_size('tp'), product...  61.7 us
    pad x16, local copies, waits for them, and re-layouts, on_device(): lax.associative_scan(combine_states, (decays, updates))  28.7 us
    convert_element_type x2, local copies, waits for them, and re-layouts, on_device(): product.reshape(rows_each * lax.axis_size('tp'), product.shape[-1])  20.4 us
    dot_general x1, matrix products, on_device(): jnp.einsum('tsecf,efd->tsecd', hidden, expert_down_weight, preferred_elem...  10.4 us
    unnamed x63, local copies, waits for them, and re-layouts  9.39 us
    add x10, other arithmetic, on_device(): lax.associative_scan(combine_states, (decays, updates))  7.64 us
    all_to_all x1, starting transfers between devices, on_device(): lax.all_to_all(outgoing, 'ep', split_axis=0, concat_axis=0, tiled=True)  7.48 us
    dot_general x1, matrix products, on_device(): jnp.einsum('tsecd,edf->tsecf', shaped, expert_up_weight, preferred_elemen...  7.46 us
  transfers between devices with their start and end apart: 6, of which 4 were waited for; matrix products, arithmetic and copies ran while one was open for 50% of the time, Pallas kernels for 0%

profile of v1, /device:TPU:2, one launch (start us, length us, event | category | flops | bytes accessed | tf_op | source)
XLA Modules:
  0.0 248.4 jit_solution(641484723890311199)
XLA Ops:
  7.2 0.9 constant_dynamic-slice_fusion.1
  9.0 0.8 scatter_custom_fusion
  9.8 1.0 fusion.61
  10.9 1.0 fusion.63
  11.9 0.8 gather_fusion
  12.9 0.9 broadcast_select_fusion
  13.9 7.5 %all-to-all-start.1 = ((bf16[16,5,2048]{2,1,0:T(8,128)(2,1)}), bf16[16,5,2048]{2,1,0:T(8,128)(2,1)S(1)}, u32[]{:S(2)}, u32[]{:S(2)}) async-start(bf16[16,5,2048]{2,1,0:T(8,128)(2,1)} %broadcast_select_fusion), calls=%async_computation.1 | async-start | bytes 1048576 | tf_op jit(solution)/shard_map/all_to_all | solution.py:180
  21.4 1.3 add_divide_fusion
  23.2 0.7 reduce.14
  24.1 0.8 fusion.37
  24.8 1.0 copy-done.2
  26.6 4.9 %all-to-all-done.1 = bf16[16,5,2048]{2,1,0:T(8,128)(2,1)S(1)} async-done(((bf16[16,5,2048]{2,1,0:T(8,128)(2,1)}), bf16[16,5,2048]{2,1,0:T(8,128)(2,1)S(1)}, u32[]{:S(2)}, u32[]{:S(2)}) %all-to-all-start.1) | async-done | bytes 327712 | tf_op jit(solution)/shard_map/all_to_all | solution.py:180
  31.5 0.9 copy.136
  33.5 0.7 copy.128
  34.2 1.5 reshape.459
  35.7 1.5 convert_multiply_fusion
  37.2 3.8 %fusion.30 = (bf16[32,64,128]{2,0,1:T(8,128)(2,1)}, bf16[32,64,128]{2,0,1:T(8,128)(2,1)}, bf16[32,64,128]{2,0,1:T(8,128)(2,1)S(1)}) fusion(f32[32,64,1,128]{3,0,1,2:T(8,128)} %copy-done.2, f32[32,64,128]{2,1,0:T(8,128)S(1)} %bitcast.157, f32[32,128]{1,0:T(8,128)S(1)} %get-tuple-element.9, f32[32,64,128]{2,1,0:T(8,128)S(1)} %bitcast.154, f32[128]{0:T(128)S(1)} %copy-done.26), kind=kLoop, calls=%fused_computation.39 | loop fusion | flops 2359296 | bytes 4735488 | tf_op jit(solution)/shard_map/mul | solution.py:149
  41.5 0.6 slice.309
  42.2 0.7 slice.310
  43.5 0.6 pad_add_fusion
  44.2 0.8 pad.67
  44.9 0.8 fusion.82
  45.7 0.6 pad_maximum_fusion.3
  46.4 2.1 pad.66
  48.4 1.6 add.231
  50.0 1.0 fusion.65
  51.0 0.8 pad_maximum_fusion.2
  51.8 2.0 pad.68
  53.7 3.5 %pad.69 = f32[8,1,128,64]{2,3,0,1:T(8,128)} pad(f32[4,1,128,64]{2,3,0,1:T(8,128)} %add.231, f32[]{:T(128)} %constant.15.clone.1), padding=1_0_1x0_0_0x0_0_0x0_0_0 | pad | bytes 393220 | tf_op jit(solution)/shard_map/pad | solution.py:139
  57.2 1.8 add.233
  59.0 5.1 %pad.71 = f32[16,1,128,64]{2,3,0,1:T(8,128)} pad(f32[8,1,128,64]{2,3,0,1:T(8,128)} %add.233, f32[]{:T(128)} %constant.15.clone.1), padding=1_0_1x0_0_0x0_0_0x0_0_0 | pad | bytes 786436 | tf_op jit(solution)/shard_map/pad | solution.py:139
  64.1 1.1 fusion.64
  65.2 3.3 %pad.70 = f32[16,1,128,64]{2,3,0,1:T(8,128)} pad(f32[8,1,128,64]{2,3,0,1:T(8,128)S(1)} %pad_maximum_fusion.1, f32[]{:T(128)} %constant.15.clone.1), padding=0_1_1x0_0_0x0_0_0x0_0_0 | pad | bytes 786436 | tf_op jit(solution)/shard_map/pad | solution.py:139
  68.5 1.3 add.235
  69.9 5.9 %pad.149 = f32[31,1,128,64]{2,3,0,1:T(8,128)} pad(f32[16,1,128,64]{2,3,0,1:T(8,128)S(1)} %add.235, f32[]{:T(128)} %constant.15.clone.1), padding=0_0_1x0_0_0x0_0_0x0_0_0 | pad | bytes 1540100
  75.8 0.8 fusion.71
  76.6 0.8 broadcast_in_dim.57
  77.4 5.4 %all-to-all-start = ((bf16[16,130,64]{1,2,0:T(8,128)(2,1)}), bf16[16,130,64]{1,2,0:T(8,128)(2,1)}, u32[]{:S(2)}, u32[]{:S(2)}) async-start(bf16[16,130,64]{1,2,0:T(8,128)(2,1)} %broadcast_in_dim.57), calls=%async_computation | async-start | bytes 1048576 | tf_op jit(solution)/shard_map/all_to_all | solution.py:15
  83.0 6.0 %pad.73 = f32[32,1,128,64]{2,3,0,1:T(8,128)} pad(f32[16,1,128,64]{2,3,0,1:T(8,128)S(1)} %add.235, f32[]{:T(128)} %constant.15.clone.1), padding=1_0_1x0_0_0x0_0_0x0_0_0 | pad | bytes 1572868 | tf_op jit(solution)/shard_map/pad | solution.py:139
  88.9 0.7 slice_bitcast_fusion.2
  89.7 1.3 fusion.58
  91.0 5.9 %pad.72 = f32[32,1,128,64]{2,3,0,1:T(8,128)} pad(f32[16,1,128,64]{2,3,0,1:T(8,128)S(1)} %pad_maximum_fusion, f32[]{:T(128)} %constant.15.clone.1), padding=0_1_1x0_0_0x0_0_0x0_0_0 | pad | bytes 1572868 | tf_op jit(solution)/shard_map/pad | solution.py:139
  97.0 2.4 slice_add_fusion
  99.4 3.2 %convolution_bitcast_fusion = f32[32,64,64]{2,1,0:T(8,128)} fusion(bf16[32,64,128]{2,0,1:T(8,128)(2,1)} %get-tuple-element.5, bf16[32,64,128]{2,0,1:T(8,128)(2,1)} %copy-done.6, pred[64,64]{1,0:T(8,128)(4,1)S(1)} %iota_compare_fusion.1, bf16[32,64,64]{1,0,2:T(8,128)(2,1)} %copy-done.7), kind=kOutput, calls=%fused_computation.23 | convolution fusion | flops 50462720 | bytes 1839104 | tf_op jit(solution)/shard_map/nhts,nshv->nthv/dot_general | solution.py:136
  102.6 1.7 slice.331
  104.3 1.1 copy.143
  105.7 1.1 select_bitcast_fusion
  107.6 0.6 copy.133
  108.6 1.8 fusion.56
  110.8 7.5 %fusion = f32[16,16,5,448]{3,1,2,0:T(8,128)} fusion(bf16[16,16,5,2048]{3,1,0,2:T(8,128)(2,1)} %bitcast.170, bf16[1,2048,448]{1,2,0:T(8,128)(2,1)} %param.28), kind=kOutput, calls=%fused_computation.5 | convolution fusion | flops 2348810240 | bytes 9371648 | tf_op jit(solution)/shard_map/tsecd,edf->tsecf/dot_general | solution.py:186
  118.2 10.4 %convert_bitcast_fusion = bf16[16,16,1,5,2048]{4,1,3,0,2:T(8,128)(2,1)} fusion(bf16[1,448,2048]{2,1,0:T(8,128)(2,1)S(1)} %copy-done, f32[16,16,5,448]{3,1,2,0:T(8,128)} %fusion, bf16[16,16,5,2048]{3,1,0,2:T(8,128)(2,1)} %bitcast.171, bf16[1,2048,448]{1,2,0:T(8,128)(2,1)} %param.27), kind=kOutput, calls=%fused_computation.4 | convolution fusion | flops 4703682560 | bytes 16449536 | tf_op jit(solution)/shard_map/tsecf,efd->tsecd/dot_general | solution.py:191
  128.6 10.4 %copy.139 = bf16[16,16,1,5,2048]{4,3,1,0,2:T(8,128)(2,1)} copy(bf16[16,16,1,5,2048]{4,1,3,0,2:T(8,128)(2,1)} %convert_bitcast_fusion) | data formatting | bytes 10485760 | tf_op jit(solution)/shard_map/convert_element_type | solution.py:195
  139.0 10.0 %convert_element_type.116 = bf16[1280,2048]{1,0:T(8,128)(2,1)} reshape(bf16[16,16,1,5,2048]{4,3,1,0,2:T(8,128)(2,1)} %copy.139) | data formatting | bytes 10485760 | tf_op jit(solution)/shard_map/convert_element_type | solution.py:195
  149.1 0.8 constant_dynamic-slice_fusion
  150.0 5.3 %all-gather.5.cloned.1.call-done = bf16[32768,64]{0,1:T(8,128)(2,1)} async-done(((bf16[2048,64]{0,1:T(8,128)(2,1)}), bf16[32768,64]{0,1:T(8,128)(2,1)}) %all-gather.5.cloned.1.call-update) | async-done | bytes 4194320 | tf_op jit(solution)/shard_map/all_gather | solution.py:159
  155.4 4.8 %copy.184 = bf16[8,16,8,2048]{3,2,0,1:T(8,128)(2,1)} copy(bf16[8,16,8,2048]{3,2,1,0:T(8,128)(2,1)} %bitcast.158) | data formatting | bytes 8388608 | tf_op jit(solution)/shard_map/all_gather | solution.py:159
  160.1 61.7 %reduce-scatter.2.cloned.1.call-done = bf16[80,2048]{1,0:T(8,128)(2,1)} async-done(((bf16[1280,2048]{1,0:T(8,128)(2,1)}), bf16[80,2048]{1,0:T(8,128)(2,1)}) %reduce-scatter.2.cloned.1.call-update) | async-done | bytes 327696 | tf_op jit(solution)/shard_map/reduce_scatter | solution.py:194
  221.8 1.9 reshape.469
  223.7 7.1 %all-to-all-start.2 = ((bf16[16,5,2048]{2,1,0:T(8,128)(2,1)}), bf16[16,5,2048]{2,1,0:T(8,128)(2,1)S(1)}, u32[]{:S(2)}, u32[]{:S(2)}) async-start(bf16[16,5,2048]{2,1,0:T(8,128)(2,1)} %reshape.469), calls=%async_computation.3 | async-start | bytes 1048576 | tf_op jit(solution)/shard_map/all_to_all | solution.py:201
  230.8 4.4 %convolution_convert_fusion = bf16[2048,128]{1,0:T(8,128)(2,1)} fusion(bf16[2048,1024]{0,1:T(8,128)(2,1)} %bitcast.159, bf16[1024,128]{1,0:T(8,128)(2,1)S(1)} %copy-done.28), kind=kOutput, calls=%fused_computation.17 | convolution fusion | flops 537133056 | bytes 4980736 | tf_op jit(solution)/shard_map/dot_general | solution.py:158
  235.3 4.3 %all-to-all-done.2 = bf16[16,5,2048]{2,1,0:T(8,128)(2,1)S(1)} async-done(((bf16[16,5,2048]{2,1,0:T(8,128)(2,1)}), bf16[16,5,2048]{2,1,0:T(8,128)(2,1)S(1)}, u32[]{:S(2)}, u32[]{:S(2)}) %all-to-all-start.2) | async-done | bytes 327712 | tf_op jit(solution)/shard_map/all_to_all | solution.py:201
  239.7 0.7 gather_fusion.1
  240.4 0.7 gather_fusion.2
  241.1 0.8 add_convert_fusion
  (166 shorter events, 6.9 us)
Async XLA Ops:
  7.2 111.1 %copy-start = (bf16[1,448,2048]{2,1,0:T(8,128)(2,1)S(1)}, bf16[1,448,2048]{2,1,0:T(8,128)(2,1)}, u32[]{:S(2)}) copy-start(bf16[1,448,2048]{2,1,0:T(8,128)(2,1)} %param.29) | copy-start | bytes 5505028
  12.7 10.5 %copy-start.25 = (f32[2048,1]{0,1:T(1,128)S(1)}, f32[2048,1]{0,1:T(1,128)}, u32[]{:S(2)}) copy-start(f32[2048,1]{0,1:T(1,128)} %param.20) | copy-start | bytes 24580
  12.7 11.4 %copy-start.26 = (f32[128]{0:T(128)S(1)}, f32[128]{0:T(128)}, u32[]{:S(2)}) copy-start(f32[128]{0:T(128)} %param.19) | copy-start | bytes 1540
  13.9 17.6 %all-to-all-start.1 = ((bf16[16,5,2048]{2,1,0:T(8,128)(2,1)}), bf16[16,5,2048]{2,1,0:T(8,128)(2,1)S(1)}, u32[]{:S(2)}, u32[]{:S(2)}) async-start(bf16[16,5,2048]{2,1,0:T(8,128)(2,1)} %broadcast_select_fusion), calls=%async_computation.1 | async-start | bytes 1048576 | tf_op jit(solution)/shard_map/all_to_all | solution.py:180
  21.3 89.4 %all-gather.7.cloned.1.call-start = ((), (), s32[]{:S(2)}) async-start(), calls=%async_computation.6 | async-start | bytes 5570560 | tf_op jit(solution)/shard_map/all_gather | solution.py:181
  24.8 1.0 copy-start.2
  26.4 14.5 %copy-start.14 = (f32[32,1,128]{2,0,1:T(8,128)}, f32[32,1,128]{2,0,1:T(8,128)S(1)}, u32[]{:S(2)}) copy-start(f32[32,1,128]{2,0,1:T(8,128)S(1)} %get-tuple-element.8) | copy-start | bytes 49156
  32.5 0.7 copy-start.24
  32.6 0.8 copy-start.23
  33.3 7.7 %copy-start.18 = (f32[16,1,128]{2,0,1:T(8,128)}, f32[16,1,128]{2,0,1:T(8,128)S(1)}, u32[]{:S(2)}) copy-start(f32[16,1,128]{2,0,1:T(8,128)S(1)} %pad.81) | copy-start | bytes 24580
  33.3 7.6 %copy-start.20 = (f32[16,1,128]{2,0,1:T(8,128)}, f32[16,1,128]{2,0,1:T(8,128)S(1)}, u32[]{:S(2)}) copy-start(f32[16,1,128]{2,0,1:T(8,128)S(1)} %pad.80) | copy-start | bytes 24580
  33.4 7.6 %copy-start.16 = (f32[16,1,128]{2,0,1:T(8,128)}, f32[16,1,128]{2,0,1:T(8,128)S(1)}, u32[]{:S(2)}) copy-start(f32[16,1,128]{2,0,1:T(8,128)S(1)} %add.241) | copy-start | bytes 24580
  35.7 5.3 %copy-start.7 = (bf16[32,64,64]{1,0,2:T(8,128)(2,1)}, bf16[32,64,64]{1,0,2:T(8,128)(2,1)S(1)}, u32[]{:S(2)}) copy-start(bf16[32,64,64]{1,0,2:T(8,128)(2,1)S(1)} %reshape.459) | copy-start | bytes 786436
  41.0 1.9 copy-start.6
  42.2 0.8 copy-start.8
  42.8 0.7 copy-start.10
  42.9 0.6 copy-start.11
  42.9 0.6 copy-start.12
  53.7 11.5 %copy-start.13 = (f32[1,1,128,64]{2,3,0,1:T(8,128)S(1)}, f32[1,1,128,64]{2,3,0,1:T(8,128)}, u32[]{:S(2)}) copy-start(f32[1,1,128,64]{2,3,0,1:T(8,128)} %slice.309) | copy-start | bytes 98308
  64.1 12.5 %copy-start.22 = (bf16[2,64]{0,1:T(8,128)(2,1)S(1)}, bf16[2,64]{0,1:T(8,128)(2,1)}, u32[]{:S(2)}) copy-start(bf16[2,64]{0,1:T(8,128)(2,1)} %copy.128) | copy-start | bytes 772
  65.2 17.7 %copy-start.15 = (f32[32,1,128]{2,0,1:T(8,128)S(1)}, f32[32,1,128]{2,0,1:T(8,128)}, u32[]{:S(2)}) copy-start(f32[32,1,128]{2,0,1:T(8,128)} %copy-done.14) | copy-start | bytes 49156
  68.5 14.4 %copy-start.17 = (f32[16,1,128]{2,0,1:T(8,128)S(1)}, f32[16,1,128]{2,0,1:T(8,128)}, u32[]{:S(2)}) copy-start(f32[16,1,128]{2,0,1:T(8,128)} %copy-done.16) | copy-start | bytes 24580
  69.8 19.8 %copy-start.19 = (f32[16,1,128]{2,0,1:T(8,128)S(1)}, f32[16,1,128]{2,0,1:T(8,128)}, u32[]{:S(2)}) copy-start(f32[16,1,128]{2,0,1:T(8,128)} %copy-done.18) | copy-start | bytes 24580
  69.8 19.8 %copy-start.21 = (f32[16,1,128]{2,0,1:T(8,128)S(1)}, f32[16,1,128]{2,0,1:T(8,128)}, u32[]{:S(2)}) copy-start(f32[16,1,128]{2,0,1:T(8,128)} %copy-done.20) | copy-start | bytes 24580
  77.4 25.2 %all-to-all-start = ((bf16[16,130,64]{1,2,0:T(8,128)(2,1)}), bf16[16,130,64]{1,2,0:T(8,128)(2,1)}, u32[]{:S(2)}, u32[]{:S(2)}) async-start(bf16[16,130,64]{1,2,0:T(8,128)(2,1)} %broadcast_in_dim.57), calls=%async_computation | async-start | bytes 1048576 | tf_op jit(solution)/shard_map/all_to_all | solution.py:15
  82.9 72.5 %all-gather.5.cloned.1.call-start = ((), (), s32[]{:S(2)}) async-start(), calls=%async_computation.5 | async-start | bytes 4456448 | tf_op jit(solution)/shard_map/all_gather | solution.py:159
  91.0 6.0 %copy-start.3 = (f32[32,1,128,64]{2,3,0,1:T(8,128)S(1)}, f32[32,1,128,64]{2,3,0,1:T(8,128)}, u32[]{:S(2)}) copy-start(f32[32,1,128,64]{2,3,0,1:T(8,128)} %pad.73) | copy-start | bytes 3145732
  99.4 7.6 %copy-start.4 = (f32[31,1,128,64]{2,3,0,1:T(8,128)S(1)}, f32[31,1,128,64]{2,3,0,1:T(8,128)}, u32[]{:S(2)}) copy-start(f32[31,1,128,64]{2,3,0,1:T(8,128)} %slice_add_fusion) | copy-start | bytes 3047428
  99.4 7.6 %copy-start.5 = (bf16[32,64,128]{2,0,1:T(8,128)(2,1)S(1)}, bf16[32,64,128]{2,0,1:T(8,128)(2,1)}, u32[]{:S(2)}) copy-start(bf16[32,64,128]{2,0,1:T(8,128)(2,1)} %get-tuple-element.4) | copy-start | bytes 1572868
  105.7 1.3 copy-start.9
  107.6 1.1 copy-start.27
  110.5 111.3 %reduce-scatter.2.cloned.1.call-start = ((), (), s32[]{:S(2)}) async-start(), calls=%async_computation.4 | async-start | bytes 5570560 | tf_op jit(solution)/shard_map/reduce_scatter | solution.py:194
  155.4 75.5 %copy-start.28 = (bf16[1024,128]{1,0:T(8,128)(2,1)S(1)}, bf16[1024,128]{1,0:T(8,128)(2,1)}, u32[]{:S(2)}) copy-start(bf16[1024,128]{1,0:T(8,128)(2,1)} %param.22) | copy-start | bytes 786436
  223.7 15.9 %all-to-all-start.2 = ((bf16[16,5,2048]{2,1,0:T(8,128)(2,1)}), bf16[16,5,2048]{2,1,0:T(8,128)(2,1)S(1)}, u32[]{:S(2)}, u32[]{:S(2)}) async-start(bf16[16,5,2048]{2,1,0:T(8,128)(2,1)} %reshape.469), calls=%async_computation.3 | async-start | bytes 1048576 | tf_op jit(solution)/shard_map/all_to_all | solution.py:201
  230.8 11.0 %copy-start.1 = (bf16[1,448,2048]{2,1,0:T(8,128)(2,1)S(1)}, bf16[1,448,2048]{2,1,0:T(8,128)(2,1)}, u32[]{:S(2)}) copy-start(bf16[1,448,2048]{2,1,0:T(8,128)(2,1)} %param.29) | copy-start | bytes 5505028
Sparse Core Ops, SparseCore 0:
  32.6 43.1 all-gather.6
  110.6 44.6 all-gather.4
  157.9 63.8 reduce-scatter.1
